TPU v7x, 32 devices: a whole 2x2x4 slice. The times are simulated.
32 devices in a mesh: sp: 4 (over z), fs: 4 (over y, x), tp: 2 (over core).
Axes of the slice: x: 2, y: 2, z: 4, core: 2. Of those that a mesh axis runs over, the one named last changes fastest.
Arguments:
- state_head_inputs: bfloat16 [4, 512, 1024], P('fs', 'sp', 'tp'), may hold values from -6 to 6
- state_write_vectors: bfloat16 [4, 512, 256], P('fs', 'sp', 'tp'), may hold values from -3 to 3
- state_read_vectors: bfloat16 [4, 512, 256], P('fs', 'sp', 'tp'), may hold values from -3 to 3
- state_output_gate: bfloat16 [4, 512, 1024], P('fs', 'sp', 'tp'), may hold values from -6 to 6
- presoftplus_steps: float32 [4, 16, 512], P('fs', 'tp', 'sp'), may hold values from -6 to 6
- extra_decay_log: float32 [4, 16, 512], P('fs', 'tp', 'sp'), may hold values from -2.1 to 0, as said below
- lane_shrinkage_powers: float32 [16], P('tp')
- bypass_coefficient_vector: float32 [16], P('tp'), may hold values from 0.5 to 4
- feeder_smoothing_stencil: bfloat16 [4, 1024], P(None, 'tp'), may hold values from -3 to 3
- stored_smoothing_stencil: bfloat16 [4, 256], P(None, 'tp'), may hold values from -3 to 3
- lookup_smoothing_stencil: bfloat16 [4, 256], P(None, 'tp'), may hold values from -3 to 3
- bundled_rescaling_vector: float32 [1024], P('tp'), may hold values from 0.1 to 1.9
- queries: bfloat16 [4, 512, 1024], P('fs', 'sp', 'tp'), may hold values from -8 to 8
- attention_keys: bfloat16 [4, 512, 256], P('fs', 'sp', 'tp'), may hold values from -8 to 8
- attention_values: bfloat16 [4, 512, 256], P('fs', 'sp', 'tp'), may hold values from -6 to 6
- forget_gate_cumsum: float32 [4, 512, 16], P('fs', 'sp', 'tp'), as said below
- state_out_weight: bfloat16 [1024, 2048], P('tp', 'fs'), may hold values from -0.1875 to 0.1875
- attention_out_weight: bfloat16 [1024, 2048], P('tp', 'fs'), may hold values from -0.75 to 0.75
Outputs:
- layer_output: bfloat16 [4, 512, 2048], P('fs', ('sp', 'tp'))
Inputs may be any that keep to these rules, and one draw needn't show every extreme that they name: `extra_decay_log`: nonpositive. `forget_gate_cumsum`: never rises along the positions of a sequence.
All inputs are finite; a program needn't handle non-finite values.
Results may differ from a plain program's by a relative error of at most 0.019.
Values may be sent and summed in bfloat16 or wider, within the bound.
A program may use at most 64 MiB of HBM per device.

v0:
```python
import math

import jax
import jax.numpy as jnp
from jax import lax
from jax.sharding import PartitionSpec as P

HEAD_DIM = 64
STATE = 128


EPSILON = 1e-06
NEGATIVE = -1e30


def passed_along(shard, axis, by):
    devices = lax.axis_size(axis)
    pairs = [(i, i + by) for i in range(devices) if 0 <= i + by < devices]
    return lax.ppermute(shard, axis, pairs)


def entering(shard, axis, join, neutral):
    place = lax.axis_index(axis)
    gathered = jax.tree.map(
        lambda a, kind: lax.all_gather(a.astype(kind), axis), shard, (jnp.bfloat16, jnp.bfloat16)
    )
    state = jax.tree.map(lambda a, e: jnp.zeros_like(a) + jnp.asarray(e, a.dtype), shard, neutral)

    def one(hop, state):
        return join(
            state,
            jax.tree.map(
                lambda a, own: lax.dynamic_index_in_dim(a, hop, 0, False).astype(own.dtype),
                gathered,
                shard,
            ),
        )

    return lax.fori_loop(0, place, one, state)


def causal_filter(feeder_quantities, before, taps):
    length = feeder_quantities.shape[0]
    padded = jnp.concatenate([before, feeder_quantities], axis=0).astype(jnp.float32)
    summed = jnp.zeros(feeder_quantities.shape, jnp.float32)
    for offset in range(taps.shape[0]):
        summed = summed + taps[offset].astype(jnp.float32) * padded[offset : offset + length]
    return jax.nn.silu(summed).astype(jnp.bfloat16)


def compose(earlier, later):
    return (earlier[0] * later[0], earlier[1] * later[0][..., None, None] + later[1])


def shards(
    state_head_inputs,
    state_write_vectors,
    state_read_vectors,
    state_output_gate,
    presoftplus_steps,
    extra_decay_log,
    lane_shrinkage_powers,
    bypass_coefficient_vector,
    feeder_smoothing_stencil,
    stored_smoothing_stencil,
    lookup_smoothing_stencil,
    bundled_rescaling_vector,
    queries,
    attention_keys,
    attention_values,
    forget_gate_cumsum,
    state_out_weight,
    attention_out_weight,
):
    shard_rows = state_head_inputs.shape[1]
    input_rows = state_head_inputs[0]
    write_rows = state_write_vectors[0]
    read_rows = state_read_vectors[0]
    tap_rows = feeder_smoothing_stencil.shape[0] - 1
    value_width = input_rows.shape[1]
    vector_width = write_rows.shape[1]
    tail_rows = jnp.concatenate(
        [input_rows[-tap_rows:], write_rows[-tap_rows:], read_rows[-tap_rows:]], axis=1
    )
    before = passed_along(tail_rows, "sp", 1)
    conv_values = causal_filter(input_rows, before[:, :value_width], feeder_smoothing_stencil)
    conv_write = causal_filter(
        write_rows, before[:, value_width : value_width + vector_width], stored_smoothing_stencil
    )
    conv_read = causal_filter(
        read_rows, before[:, value_width + vector_width :], lookup_smoothing_stencil
    )
    stride_duration = jax.nn.softplus(presoftplus_steps[0])
    shrinkage_natural_power = (
        stride_duration * (-jnp.exp(lane_shrinkage_powers))[:, None] + extra_decay_log[0]
    )
    lane_tally = stride_duration.shape[0]
    groups = vector_width // STATE
    per_group = lane_tally // groups
    cumulative = jnp.cumsum(shrinkage_natural_power, axis=1)
    input_heads = conv_values.reshape(shard_rows, groups, per_group, HEAD_DIM)
    write_groups = conv_write.reshape(shard_rows, groups, STATE)
    read_groups = conv_read.reshape(shard_rows, groups, STATE)
    inner_products = jnp.einsum(
        "tgn,sgn->gts", read_groups, write_groups, preferred_element_type=jnp.float32
    )
    positions = jnp.arange(shard_rows)
    causal = positions[:, None] >= positions[None, :]
    log_gap = jnp.where(causal[None], cumulative[:, :, None] - cumulative[:, None, :], -jnp.inf)
    weights = jnp.exp(log_gap) * stride_duration[:, None, :]
    mix_weights = (
        inner_products[:, None] * weights.reshape(groups, per_group, shard_rows, shard_rows)
    ).astype(jnp.bfloat16)
    local_part = jnp.einsum(
        "ghts,sghp->tghp", mix_weights, input_heads, preferred_element_type=jnp.float32
    )
    end_scale = (jnp.exp(cumulative[:, -1:] - cumulative) * stride_duration).T.reshape(
        shard_rows, groups, per_group
    )
    weighted = (input_heads.astype(jnp.float32) * end_scale[..., None]).astype(jnp.bfloat16)
    block_state = jnp.einsum(
        "sghp,sgn->ghpn", weighted, write_groups, preferred_element_type=jnp.float32
    )
    total_decay = jnp.exp(cumulative[:, -1]).reshape(groups, per_group)
    identity = (jnp.ones_like(total_decay), jnp.zeros_like(block_state))
    carried = entering((total_decay, block_state), "sp", compose, identity)[1]
    carried_part = jnp.einsum(
        "tgn,ghpn->tghp",
        read_groups,
        carried.astype(jnp.bfloat16),
        preferred_element_type=jnp.float32,
    )
    carried_part = (
        carried_part * jnp.exp(cumulative).T.reshape(shard_rows, groups, per_group)[..., None]
    )
    mixer_sum = (
        local_part
        + carried_part
        + bypass_coefficient_vector.reshape(groups, per_group)[None, :, :, None]
        * input_heads.astype(jnp.float32)
    )
    gated_rows = mixer_sum.reshape(shard_rows, groups, per_group * HEAD_DIM) * jax.nn.silu(
        state_output_gate[0].astype(jnp.float32)
    ).reshape(shard_rows, groups, -1)
    stretch_coefficient = lax.rsqrt(
        jnp.mean(gated_rows * gated_rows, axis=-1, keepdims=True) + EPSILON
    )
    state_result = (
        (gated_rows * stretch_coefficient * bundled_rescaling_vector.reshape(groups, -1))
        .reshape(shard_rows, -1)
        .astype(jnp.bfloat16)
    )
    attend_heads = forget_gate_cumsum.shape[2]
    key_group_count = attention_keys.shape[2] // HEAD_DIM
    repeat_factor = attend_heads // key_group_count
    query_head_count = queries[0].reshape(shard_rows, key_group_count, repeat_factor, HEAD_DIM)
    first_query = lax.axis_index("sp") * shard_rows
    query_index = first_query + jnp.arange(shard_rows)
    last_query = first_query + shard_rows - 1
    query_gates = forget_gate_cumsum[0].T
    all_gates = lax.all_gather(forget_gate_cumsum[0], "sp", axis=0, tiled=True)
    attention_score_scale = HEAD_DIM ** (-0.5)
    starting = (
        jnp.full((attend_heads, shard_rows), NEGATIVE, jnp.float32),
        jnp.zeros((attend_heads, shard_rows), jnp.float32),
        jnp.zeros((attend_heads, shard_rows, HEAD_DIM), jnp.float32),
    )
    key_rows = lax.all_gather(attention_keys[0], "sp", axis=0, tiled=True)
    value_rows = lax.all_gather(attention_values[0], "sp", axis=0, tiled=True)
    span = key_rows.shape[0]
    sub_block = math.gcd(span, 512)

    def advance(sub_index, running):
        first_key = sub_index * sub_block

        def attend(running):
            running_max, running_sum, weighted_sum = running
            key_tile = lax.dynamic_slice_in_dim(
                key_rows, sub_index * sub_block, sub_block, 0
            ).reshape(sub_block, key_group_count, HEAD_DIM)
            value_tile = lax.dynamic_slice_in_dim(
                value_rows, sub_index * sub_block, sub_block, 0
            ).reshape(sub_block, key_group_count, HEAD_DIM)
            key_gates = lax.dynamic_slice_in_dim(all_gates, first_key, sub_block, 0)
            attention_scores = jnp.einsum(
                "ezxp,czp->zxec", query_head_count, key_tile, preferred_element_type=jnp.float32
            )
            attention_scores = (
                attention_scores.reshape(attend_heads, shard_rows, sub_block)
                * attention_score_scale
            )
            attention_scores = attention_scores + query_gates[:, :, None] - key_gates.T[:, None, :]
            visible = (first_key + jnp.arange(sub_block))[None, :] <= query_index[:, None]
            attention_scores = jnp.where(visible[None], attention_scores, NEGATIVE)
            new_max = jnp.maximum(running_max, jnp.max(attention_scores, axis=-1))
            shrink = jnp.exp(running_max - new_max)
            attention_probs = jnp.where(
                visible[None], jnp.exp(attention_scores - new_max[..., None]), 0.0
            )
            running_sum = running_sum * shrink + jnp.sum(attention_probs, axis=-1)
            weighted_value_sum = jnp.einsum(
                "fljx,xfc->fljc",
                attention_probs.astype(jnp.bfloat16).reshape(
                    key_group_count, repeat_factor, shard_rows, sub_block
                ),
                value_tile,
                preferred_element_type=jnp.float32,
            )
            weighted_sum = weighted_sum * shrink[..., None] + weighted_value_sum.reshape(
                attend_heads, shard_rows, HEAD_DIM
            )
            return (new_max, running_sum, weighted_sum)

        return lax.cond(first_key <= last_query, attend, lambda kept: kept, running)

    _, running_sum, weighted_sum = lax.fori_loop(0, span // sub_block, advance, starting)
    attend_out = (
        (weighted_sum / running_sum[..., None])
        .transpose(1, 0, 2)
        .reshape(shard_rows, -1)
        .astype(jnp.bfloat16)
    )
    state_columns, attend_columns = (
        lax.all_gather(state_out_weight, "fs", axis=1, tiled=True),
        lax.all_gather(attention_out_weight, "fs", axis=1, tiled=True),
    )
    summed = lax.psum_scatter(
        (
            jnp.dot(state_result, state_columns, preferred_element_type=jnp.float32)
            + jnp.dot(attend_out, attend_columns, preferred_element_type=jnp.float32)
        ).astype(jnp.bfloat16),
        "tp",
        scatter_dimension=0,
        tiled=True,
    )
    return summed[None]


def solution(mesh):
    in_specs = (
        P("fs", "sp", "tp"),
        P("fs", "sp", "tp"),
        P("fs", "sp", "tp"),
        P("fs", "sp", "tp"),
        P("fs", "tp", "sp"),
        P("fs", "tp", "sp"),
        P("tp"),
        P("tp"),
        P(None, "tp"),
        P(None, "tp"),
        P(None, "tp"),
        P("tp"),
        P("fs", "sp", "tp"),
        P("fs", "sp", "tp"),
        P("fs", "sp", "tp"),
        P("fs", "sp", "tp"),
        P("tp", "fs"),
        P("tp", "fs"),
    )
    out_specs = P("fs", ("sp", "tp"), None)
    return jax.shard_map(shards, mesh=mesh, in_specs=in_specs, out_specs=out_specs, check_vma=False)
```

profile of v0, /device:TPU:25, one launch (start us, length us, event | category | flops | bytes accessed | tf_op | source)
XLA Modules:
  0.0 107.5 jit_solution(7209099858633542223)
XLA Ops:
  6.5 0.7 all-gather.8.cloned.1.call-update
  7.3 0.0 all-gather.10.cloned.1.call-start
  7.3 0.7 slice_bitcast_fusion.1
  8.0 0.7 slice_bitcast_fusion
  8.7 0.2 copy.46
  8.9 1.3 %collective-permute-start = (bf16[3,768]{0,1:T(8,128)(2,1)S(1)}, bf16[3,768]{0,1:T(8,128)(2,1)S(1)}, u32[]{:S(2)}, u32[]{:S(2)}) collective-permute-start(bf16[3,768]{0,1:T(8,128)(2,1)S(1)} %copy.46), channel_id=1, source_target_pairs={{0,8},{8,16},{16,24},{1,9},{9,17},{17,25},{2,10},{10,18},{18,26},{... | collective-permute-start | bytes 13832 | tf_op jit(solution)/shard_map/ppermute | solution.py:19
  10.2 0.0 all-gather.10.cloned.1.call-update
  10.2 0.0 reduce-scatter.2.cloned.1.call-start
  10.3 0.7 exponential_negate_fusion
  11.0 0.8 compare_select_fusion
  11.7 0.3 reduce_window_sum.11
  12.0 0.2 slice_reduce_fusion
  12.2 0.8 multiply_bitcast_fusion
  13.0 0.9 slice_convert_fusion.3
  13.8 0.8 bitcast_convert_fusion.4
  14.7 0.8 bitcast_convert_fusion.8
  15.5 0.9 copy.53
  16.4 9.7 %all-gather.2 = bf16[1,512,128]{1,2,0:T(8,128)(2,1)S(1)} all-gather(bf16[1,128,128]{1,2,0:T(8,128)(2,1)S(1)} %copy.53), channel_id=4, replica_groups=mesh['sp'=4,'fs'=4,'tp'=2] {'sp'}, dimensions={1}, use_global_device_ids=true | all-gather | bytes 163840 | tf_op jit(solution)/shard_map/all_gather | solution.py:168
  26.1 10.5 %all-gather.3 = f32[1,512,8]{1,2,0:T(8,128)S(1)} all-gather(f32[1,128,8]{1,2,0:T(8,128)} %param.37), channel_id=5, replica_groups=mesh['sp'=4,'fs'=4,'tp'=2] {'sp'}, dimensions={1}, use_global_device_ids=true | all-gather | bytes 20480 | tf_op jit(solution)/shard_map/all_gather | solution.py:161
  36.5 0.9 copy.54
  37.4 9.5 %all-gather.4 = bf16[1,512,128]{1,2,0:T(8,128)(2,1)S(1)} all-gather(bf16[1,128,128]{1,2,0:T(8,128)(2,1)S(1)} %copy.54), channel_id=6, replica_groups=mesh['sp'=4,'fs'=4,'tp'=2] {'sp'}, dimensions={1}, use_global_device_ids=true | all-gather | bytes 163840 | tf_op jit(solution)/shard_map/all_gather | solution.py:169
  46.9 0.0 copy-start
  46.9 0.0 copy-start.8
  46.9 0.0 copy-start.2
  46.9 1.9 %conditional.1 = ((f32[8,128]{1,0:T(8,128)S(1)}, f32[8,128,64]{1,2,0:T(8,128)S(1)})) conditional(s32[]{:T(128)} %convert_element_type.195, (f32[8,128]{1,0:T(8,128)S(1)}, f32[8,128,64]{1,2,0:T(8,128)S(1)}) %tuple.33, (s32[]{:T(128)}, s32[128]{0:T(128)S(1)}, bf16[512,128]{0,1:T(8,128)(2,1)S(1)}, bf16[1,128,512]{2,1,0:T(8,128)(2,1)S(1)}, ...), branch_computations={%region_4.5_spmd, %region_5.8_spmd} | conditional | flops 140183680 | bytes 8361500 | solution.py:214
  47.0 0.1 copy.55
  47.2 0.8 fusion.47
  47.9 0.4 fusion.3
  48.3 0.5 fusion.4
  48.8 0.1 bitcast_add_fusion.1
  48.9 0.0 copy-start.3
  48.9 0.2 fusion.45
  49.1 0.1 copy.47
  49.3 0.0 copy-done.8
  49.3 0.6 dynamic-slice
  50.5 0.2 dynamic-update-slice
  50.7 8.3 %all-reduce = bf16[32]{0:T(256)(128)(2,1)S(1)} all-reduce(bf16[32]{0:T(256)(128)(2,1)S(1)} %dynamic-update-slice), channel_id=2, replica_groups=mesh['sp'=4,'fs'=4,'tp'=2] {'sp'}, use_global_device_ids=true, to_apply=%add | all-reduce | flops 32 | bytes 128
  59.0 0.1 reshape.369
  59.0 0.1 copy.52
  59.2 0.0 collective-permute-done
  59.2 0.1 copy.49
  59.3 0.1 maximum_convert_fusion
  59.5 0.1 multiply_convert_fusion.3
  59.5 0.6 fusion.23
  60.1 0.2 convolution_convert_fusion
  60.3 12.0 %all-gather.1 = bf16[32,64,128]{2,1,0:T(8,128)(2,1)S(1)} all-gather(bf16[8,64,128]{2,1,0:T(8,128)(2,1)S(1)} %convolution_convert_fusion), channel_id=3, replica_groups=mesh['sp'=4,'fs'=4,'tp'=2] {'sp'}, dimensions={0}, use_global_device_ids=true | all-gather | bytes 655360 | tf_op jit(solution)/shard_map/all_gather | solution.py:25
  72.3 0.1 copy.48
  72.4 0.1 multiply_convert_fusion.4
  72.5 0.1 fusion.49
  72.7 0.5 while.3
  72.7 0.1 convert_add_fusion.2
  72.9 0.1 convert_add_fusion.2
  73.0 0.1 convert_add_fusion.2
  73.1 0.0 copy-start.6
  73.1 0.2 fusion.13
  73.3 0.4 multiply_reduce_fusion
  73.8 0.1 copy-done.6
  73.8 0.1 fusion.29
  74.0 0.0 all-gather.8.cloned.1.call-done
  74.0 2.1 %fusion.50 = f32[128,2048]{1,0:T(8,128)S(1)} fusion(bf16[128,512]{0,1:T(8,128)(2,1)S(1)} %fusion.29, bf16[512,2048]{1,0:T(8,128)(2,1)} %all-gather.8.cloned.1.call-done), kind=kOutput, calls=%fused_computation.114 | convolution fusion | flops 268435456 | bytes 3276800 | tf_op jit(solution)/shard_map/dot_general | solution.py:229
  76.0 5.9 %all-gather.10.cloned.1.call-done = bf16[512,2048]{1,0:T(8,128)(2,1)} async-done(((bf16[512,512]{1,0:T(8,128)(2,1)}), bf16[512,2048]{1,0:T(8,128)(2,1)}) %all-gather.10.cloned.1.call-update) | async-done | bytes 2097168 | tf_op jit(solution)/shard_map/all_gather | solution.py:225
  81.9 2.9 %fusion.10 = bf16[128,2048]{1,0:T(8,128)(2,1)} fusion(f32[128,2048]{1,0:T(8,128)S(1)} %fusion.50, bf16[128,512]{0,1:T(8,128)(2,1)S(1)} %bitcast.183, bf16[512,2048]{1,0:T(8,128)(2,1)} %all-gather.10.cloned.1.call-done), kind=kOutput, calls=%fused_computation.20 | convolution fusion | flops 268959744 | bytes 3801088 | tf_op jit(solution)/shard_map/dot_general | solution.py:230
  84.8 0.0 reduce-scatter.2.cloned.1.call-update
  84.8 16.1 %reduce-scatter.2.cloned.1.call-done = bf16[64,2048]{1,0:T(8,128)(2,1)} async-done(((bf16[128,2048]{1,0:T(8,128)(2,1)}), bf16[64,2048]{1,0:T(8,128)(2,1)}) %reduce-scatter.2.cloned.1.call-update) | async-done | bytes 262160 | tf_op jit(solution)/shard_map/reduce_scatter | solution.py:227
  (33 shorter events, 0.3 us)
Async XLA Ops:
  6.5 40.3 %copy-start.5 = (f32[1,128,8]{1,2,0:T(8,128)S(1)}, f32[1,128,8]{1,2,0:T(8,128)}, u32[]{:S(2)}) copy-start(f32[1,128,8]{1,2,0:T(8,128)} %param.37) | copy-start | bytes 12292
  6.5 40.4 %copy-start.1 = (bf16[1,128,512]{2,1,0:T(8,128)(2,1)S(1)}, bf16[1,128,512]{2,1,0:T(8,128)(2,1)}, u32[]{:S(2)}) copy-start(bf16[1,128,512]{2,1,0:T(8,128)(2,1)} %param.34) | copy-start | bytes 393220
  6.5 67.4 %all-gather.8.cloned.1.call-start = ((), (), s32[]{:S(2)}) async-start(), calls=%async_computation.1 | async-start | bytes 2621440 | tf_op jit(solution)/shard_map/all_gather | solution.py:224
  7.3 74.7 %all-gather.10.cloned.1.call-start = ((), (), s32[]{:S(2)}) async-start(), calls=%async_computation.2 | async-start | bytes 2621440 | tf_op jit(solution)/shard_map/all_gather | solution.py:225
  8.9 50.3 %collective-permute-start = (bf16[3,768]{0,1:T(8,128)(2,1)S(1)}, bf16[3,768]{0,1:T(8,128)(2,1)S(1)}, u32[]{:S(2)}, u32[]{:S(2)}) collective-permute-start(bf16[3,768]{0,1:T(8,128)(2,1)S(1)} %copy.46), channel_id=1, source_target_pairs={{0,8},{8,16},{16,24},{1,9},{9,17},{17,25},{2,10},{10,18},{18,26},{... | collective-permute-start | bytes 13832 | tf_op jit(solution)/shard_map/ppermute | solution.py:19
  10.2 90.7 %reduce-scatter.2.cloned.1.call-start = ((), (), s32[]{:S(2)}) async-start(), calls=%async_computation.3 | async-start | bytes 786432 | tf_op jit(solution)/shard_map/reduce_scatter | solution.py:227
  46.9 2.2 %copy-start = (bf16[1,128,512]{2,1,0:T(8,128)(2,1)S(1)}, bf16[1,128,512]{2,1,0:T(8,128)(2,1)}, u32[]{:S(2)}) copy-start(bf16[1,128,512]{2,1,0:T(8,128)(2,1)} %param.22) | copy-start | bytes 393220
  46.9 2.4 %copy-start.8 = (u32[32]{0:T(128)S(1)}, u32[32]{0:T(128)}, u32[]{:S(2)}) copy-start(u32[32]{0:T(128)} %constant.96) | copy-start | bytes 388
  46.9 12.1 %copy-start.2 = (bf16[1,128,512]{2,1,0:T(8,128)(2,1)S(1)}, bf16[1,128,512]{2,1,0:T(8,128)(2,1)}, u32[]{:S(2)}) copy-start(bf16[1,128,512]{2,1,0:T(8,128)(2,1)} %param.25) | copy-start | bytes 393220
  48.9 10.6 %copy-start.3 = (bf16[1,128,128]{2,1,0:T(8,128)(2,1)S(1)}, bf16[1,128,128]{2,1,0:T(8,128)(2,1)}, u32[]{:S(2)}) copy-start(bf16[1,128,128]{2,1,0:T(8,128)(2,1)} %param.23) | copy-start | bytes 98308
  59.0 13.3 %copy-start.4 = (bf16[1,128,128]{2,1,0:T(8,128)(2,1)S(1)}, bf16[1,128,128]{2,1,0:T(8,128)(2,1)}, u32[]{:S(2)}) copy-start(bf16[1,128,128]{2,1,0:T(8,128)(2,1)} %param.24) | copy-start | bytes 98308
  72.6 0.7 copy-start.7
  73.1 0.7 copy-start.6
Sparse Core Ops, SparseCore 0:
  9.2 35.8 all-gather.7
  46.9 35.0 all-gather.9
  85.0 15.9 reduce-scatter.1
where the time goes:
time: 109 us; the launch traced here: 107 us
  blocking collectives  49.9 us (46%)
  waiting for transfers between devices  22.8 us (21%)
  between operations  14 us (13%)
  other arithmetic  7.12 us (7%)
  matrix products  7.04 us (6%)
  local copies, waits for them, and re-layouts  5.14 us (5%)
  starting transfers between devices  1.37 us (1%)
    reduce_scatter x1, waiting for transfers between devices, shards(): lax.psum_scatter((jnp.dot(state_result, state_columns, preferred_element_...  16.1 us
    all_gather x1, blocking collectives, entering(): lax.all_gather(a.astype(kind), axis)  12 us
    all_gather x1, blocking collectives, shards(): all_gates = lax.all_gather(forget_gate_cumsum[0], 'sp', axis=0, tiled=True)  10.5 us
    all_gather x1, blocking collectives, shards(): key_rows = lax.all_gather(attention_keys[0], 'sp', axis=0, tiled=True)  9.71 us
    all_gather x1, blocking collectives, shards(): value_rows = lax.all_gather(attention_values[0], 'sp', axis=0, tiled=True)  9.46 us
    unnamed x1, blocking collectives  8.25 us
    all_gather x1, waiting for transfers between devices, shards(): lax.all_gather(attention_out_weight, 'fs', axis=1, tiled=True)  5.9 us
    unnamed x25, local copies, waits for them, and re-layouts  2.9 us
  transfers between devices with their start and end apart: 4, of which 2 were waited for; matrix products, arithmetic and copies ran while one was open for 15% of the time, Pallas kernels for 0%

commit v1 on v0

--- a/solution.py
+++ b/solution.py
@@ -1,8 +1,11 @@
+import functools
 import math
 
 import jax
 import jax.numpy as jnp
 from jax import lax
+from jax.experimental import pallas as pl
+from jax.experimental.pallas import tpu as pltpu
 from jax.sharding import PartitionSpec as P
 
 HEAD_DIM = 64
@@ -236,6 +239,465 @@
     return summed[None]
 
 
+MESH = pl.DeviceIdType.MESH
+LANES = 128
+BF16, F32 = jnp.bfloat16, jnp.float32
+
+
+def mixer_kernel(
+    sp,
+    fs,
+    x_ref,
+    w_ref,
+    r_ref,
+    gate_ref,
+    step_ref,
+    extra_ref,
+    shrink_ref,
+    bypass_ref,
+    tapx_ref,
+    tapw_ref,
+    tapr_ref,
+    gain_ref,
+    q_ref,
+    k_ref,
+    v_ref,
+    forget_ref,
+    wst_ref,
+    wat_ref,
+    out_ref,
+    pad_ref,
+    tailx,
+    tailw,
+    tailr,
+    kall,
+    vall,
+    gall,
+    qs,
+    states,
+    decays,
+    carried,
+    mix,
+    acts,
+    acc,
+    half_out,
+    half_in,
+    sums,
+    landed,
+    tail_send,
+    tail_recv,
+    kv_send,
+    kv_recv,
+    st_send,
+    st_recv,
+    act_send,
+    act_recv,
+    half_send,
+    half_recv,
+    sum_send,
+    sum_recv,
+):
+    me = lax.axis_index("sp")
+    f = lax.axis_index("fs")
+    t = lax.axis_index("tp")
+    rows, width = x_ref.shape[1], x_ref.shape[2]
+    heads = step_ref.shape[1]
+    kv_heads = k_ref.shape[2] // HEAD_DIM
+    repeat = heads // kv_heads
+    pairs = heads // 2
+    taps = tapx_ref.shape[0]
+    cols = wst_ref.shape[1]
+    half = rows // 2
+
+    barrier = pltpu.get_barrier_semaphore()
+    for d in range(1, sp):
+        pl.semaphore_signal(
+            barrier, inc=1, device_id={"sp": lax.rem(me + d, sp)}, device_id_type=MESH
+        )
+    for d in range(1, fs):
+        pl.semaphore_signal(
+            barrier, inc=1, device_id={"fs": lax.rem(f + d, fs)}, device_id_type=MESH
+        )
+    pl.semaphore_signal(barrier, inc=1, device_id={"tp": 1 - t}, device_id_type=MESH)
+
+    def remote(src, dst, send, recv, where):
+        return pltpu.make_async_remote_copy(
+            src_ref=src,
+            dst_ref=dst,
+            send_sem=send,
+            recv_sem=recv,
+            device_id=where,
+            device_id_type=MESH,
+        )
+
+    gall[me] = forget_ref[0].T
+    kall[me] = k_ref[0]
+    vall[me] = v_ref[0]
+    pl.semaphore_wait(barrier, sp - 1 + fs - 1 + 1)
+
+    tail = [
+        remote(
+            src.at[0, rows - 16 : rows, :],
+            dst,
+            tail_send.at[i],
+            tail_recv.at[i],
+            {"sp": lax.rem(me + 1, sp)},
+        )
+        for i, (src, dst) in enumerate(((x_ref, tailx), (w_ref, tailw), (r_ref, tailr)))
+    ]
+
+    @pl.when(me < sp - 1)
+    def _():
+        for copy in tail:
+            copy.start()
+
+    def kv_copies(d, source):
+        there = {"sp": lax.rem(me + d, sp)}
+        return [
+            remote(src, dst.at[source], kv_send.at[d, i], kv_recv.at[source, i], there)
+            for i, (src, dst) in enumerate(
+                ((k_ref.at[0], kall), (v_ref.at[0], vall), (gall.at[me], gall))
+            )
+        ]
+
+    for d in range(1, sp):
+
+        @pl.when(me + d < sp)
+        def _(d=d):
+            for copy in kv_copies(d, me):
+                copy.start()
+
+    lane = lax.broadcasted_iota(jnp.int32, (1, LANES), 1)
+    low = lane < HEAD_DIM
+    row_id = lax.broadcasted_iota(jnp.int32, (rows, rows), 0)
+    col_id = lax.broadcasted_iota(jnp.int32, (rows, rows), 1)
+
+    for j in range(1, sp):
+
+        @pl.when(j > me)
+        def _(j=j):
+            kall[j] = jnp.zeros(kall.shape[1:], BF16)
+            vall[j] = jnp.zeros(vall.shape[1:], BF16)
+            gall[j] = jnp.zeros(gall.shape[1:], F32)
+
+    for h in range(heads):
+        kv = h // repeat
+        piece = (q_ref[0, :, h * HEAD_DIM : (h + 1) * HEAD_DIM].astype(F32) * HEAD_DIM**-0.5).astype(
+            BF16
+        )
+        zero = jnp.zeros((rows, HEAD_DIM), BF16)
+        parts = [piece if i == kv else zero for i in range(kv_heads)]
+        qs[kv, (h % repeat) * rows : (h % repeat + 1) * rows, :] = jnp.concatenate(parts, axis=1)
+
+    head_row = lax.broadcasted_iota(jnp.int32, (heads, rows), 0)
+    power = jnp.zeros((heads, rows), F32)
+    for h in range(heads):
+        power = jnp.where(head_row == h, shrink_ref[h], power)
+    presoft = step_ref[0]
+    step = jnp.maximum(presoft, 0.0) + jnp.log1p(jnp.exp(-jnp.abs(presoft)))
+    log_decay = extra_ref[0] - jnp.exp(power) * step
+    upper = (row_id <= col_id).astype(F32)
+    cum = jnp.dot(log_decay, upper, precision=lax.Precision.HIGHEST, preferred_element_type=F32)
+    cum_end = cum[:, rows - 1 : rows]
+    end_scale = (jnp.exp(cum_end - cum) * step).T
+    exp_cum = jnp.exp(cum).T
+    cum_col = cum.T
+    decays[me] = jnp.broadcast_to(jnp.exp(cum_end), (heads, LANES))
+
+    @pl.when(me > 0)
+    def _():
+        for copy in tail:
+            copy.wait_recv()
+
+    def filtered(ref, tail_ref, tap_ref, n):
+        before = jnp.where(me > 0, tail_ref[...].astype(F32)[8:16], 0.0)
+        pad_ref[0:8, 0:n] = before
+        pad_ref[8 : 8 + rows, 0:n] = ref[0].astype(F32)
+        total = jnp.zeros((rows, n), F32)
+        for i in range(taps):
+            at = 8 - (taps - 1) + i
+            total = total + tap_ref[i : i + 1, :].astype(F32) * pad_ref[at : at + rows, 0:n]
+        return (total * jax.nn.sigmoid(total)).astype(BF16)
+
+    conv_write = filtered(w_ref, tailw, tapw_ref, STATE)
+    conv_values = filtered(x_ref, tailx, tapx_ref, width)
+
+    def expand(columns, j):
+        return jnp.where(low, columns[:, 2 * j : 2 * j + 1], columns[:, 2 * j + 1 : 2 * j + 2])
+
+    weighted = jnp.concatenate(
+        [
+            (
+                conv_values[:, j * LANES : (j + 1) * LANES].astype(F32) * expand(end_scale, j)
+            ).astype(BF16)
+            for j in range(pairs)
+        ],
+        axis=1,
+    )
+    states[me] = lax.dot_general(
+        conv_write, weighted, (((0,), (0,)), ((), ())), preferred_element_type=F32
+    ).astype(BF16)
+
+    def st_copies(d, source):
+        there = {"sp": lax.rem(me + d, sp)}
+        return [
+            remote(buf.at[source], buf.at[source], st_send.at[d, i], st_recv.at[source, i], there)
+            for i, buf in enumerate((states, decays))
+        ]
+
+    for d in range(1, sp):
+
+        @pl.when(me + d < sp)
+        def _(d=d):
+            for copy in st_copies(d, me):
+                copy.start()
+
+    conv_read = filtered(r_ref, tailr, tapr_ref, STATE)
+    inner = lax.dot_general(
+        conv_read, conv_write, (((1,), (1,)), ((), ())), preferred_element_type=F32
+    )
+    causal = row_id >= col_id
+    for j in range(pairs):
+        tile = conv_values[:, j * LANES : (j + 1) * LANES]
+        parts = []
+        for h in (2 * j, 2 * j + 1):
+            gap = jnp.where(causal, cum_col[:, h : h + 1] - cum[h : h + 1, :], NEGATIVE)
+            weights = (inner * (jnp.exp(gap) * step[h : h + 1, :])).astype(BF16)
+            parts.append(jnp.dot(weights, tile, preferred_element_type=F32))
+        bypass = jnp.where(low, bypass_ref[2 * j], bypass_ref[2 * j + 1])
+        mix[:, j * LANES : (j + 1) * LANES] = (
+            jnp.where(low, parts[0], parts[1]) + bypass * tile.astype(F32)
+        )
+
+    for j in range(sp - 1):
+
+        @pl.when(j < me)
+        def _(j=j):
+            for copy in kv_copies(1, j):
+                copy.wait_recv()
+
+    keys = kall[...].reshape(sp * rows, -1)
+    values = vall[...].reshape(sp * rows, -1)
+    visible = [j * rows + col_id <= me * rows + row_id for j in range(sp)]
+    for kv in range(kv_heads):
+        own = lane // HEAD_DIM == kv
+        summed_values = jnp.where(own, values, jnp.ones_like(values))
+        scores = lax.dot_general(
+            qs[kv], keys, (((1,), (1,)), ((), ())), preferred_element_type=F32
+        )
+        outs = []
+        for i in range(repeat):
+            h = kv * repeat + i
+            gate_col = forget_ref[0, :, h : h + 1]
+            tiles = [
+                jnp.where(
+                    visible[j],
+                    scores[i * rows : (i + 1) * rows, j * rows : (j + 1) * rows]
+                    + (gate_col - gall[j, h : h + 1, :]),
+                    NEGATIVE,
+                )
+                for j in range(sp)
+            ]
+            top = tiles[0]
+            for tile in tiles[1:]:
+                top = jnp.maximum(top, tile)
+            top = jnp.max(top, axis=1, keepdims=True)
+            probs = jnp.concatenate([jnp.exp(tile - top).astype(BF16) for tile in tiles], axis=1)
+            both = jnp.dot(probs, summed_values, preferred_element_type=F32)
+            turned = pltpu.roll(both, HEAD_DIM, 1)
+            outs.append(both / turned if h % 2 == kv else turned / both)
+        for i in range(0, repeat, 2):
+            h = kv * repeat + i
+            acts[0, 0, :, h * HEAD_DIM : (h + 2) * HEAD_DIM] = jnp.where(
+                low, outs[i], outs[i + 1]
+            ).astype(BF16)
+
+    def act_copy(kind, origin, hop):
+        return remote(
+            acts.at[kind, origin],
+            acts.at[kind, origin ^ hop],
+            act_send.at[kind, origin ^ hop],
+            act_recv.at[kind, origin ^ hop],
+            {"fs": lax.rem(f + 0, fs) ^ hop},
+        )
+
+    act_copy(0, 0, 1).start()
+    act_copy(0, 0, 2).start()
+    acc[0] = jnp.dot(acts[0, 0], wat_ref[...], preferred_element_type=F32)
+    act_copy(0, 0, 1).wait_recv()
+    act_copy(0, 1, 2).start()
+    acc[1] = jnp.dot(acts[0, 1], wat_ref[...], preferred_element_type=F32)
+
+    carried[...] = jnp.zeros(carried.shape, F32)
+    for j in range(sp - 1):
+
+        @pl.when(j < me)
+        def _(j=j):
+            for copy in st_copies(1, j):
+                copy.wait_recv()
+            for p in range(pairs):
+                at = slice(p * LANES, (p + 1) * LANES)
+                decay = jnp.where(
+                    low, decays[j, 2 * p : 2 * p + 1, :], decays[j, 2 * p + 1 : 2 * p + 2, :]
+                )
+                carried[:, at] = carried[:, at] * decay + states[j, :, at].astype(F32)
+
+    entered = jnp.dot(conv_read, carried[...].astype(BF16), preferred_element_type=F32)
+    squares = jnp.zeros((rows, LANES), F32)
+    gated = []
+    for p in range(pairs):
+        at = slice(p * LANES, (p + 1) * LANES)
+        gate = gate_ref[0, :, at].astype(F32)
+        u = (mix[:, at] + entered[:, at] * expand(exp_cum, p)) * (gate * jax.nn.sigmoid(gate))
+        gated.append(u)
+        squares = squares + u * u
+    scale = lax.rsqrt(jnp.sum(squares, axis=1, keepdims=True) / width + EPSILON)
+    for p in range(pairs):
+        at = slice(p * LANES, (p + 1) * LANES)
+        acts[1, 0, :, at] = (gated[p] * scale * gain_ref[0:1, at]).astype(BF16)
+    act_copy(1, 0, 2).start()
+    act_copy(1, 0, 1).start()
+
+    def half_copy(d):
+        return remote(
+            half_out.at[d], half_in.at[d], half_send.at[d], half_recv.at[d], {"tp": 1 - t}
+        )
+
+    def give(d):
+        there = pl.ds(pl.multiple_of((1 - t) * half, half), half)
+        half_out[d] = acc[d, there, :].astype(BF16)
+        half_copy(d).start()
+
+    def sum_copy(d):
+        return remote(sums.at[d], landed.at[d], sum_send.at[d], sum_recv.at[d], {"fs": f ^ d})
+
+    def finish(d):
+        half_copy(d).wait_recv()
+        here = pl.ds(pl.multiple_of(t * half, half), half)
+        total = (acc[d, here, :] + half_in[d].astype(F32)).astype(BF16)
+        if d:
+            sums[d] = total
+            sum_copy(d).start()
+        else:
+            out_ref[0, :, pl.ds(pl.multiple_of(f * cols, cols), cols)] = total
+
+    acc[0] += jnp.dot(acts[1, 0], wst_ref[...], preferred_element_type=F32)
+    give(0)
+    act_copy(0, 0, 2).wait_recv()
+    acc[2] = jnp.dot(acts[0, 2], wat_ref[...], preferred_element_type=F32)
+    act_copy(0, 1, 2).wait_recv()
+    acc[3] = jnp.dot(acts[0, 3], wat_ref[...], preferred_element_type=F32)
+    act_copy(1, 0, 2).wait_recv()
+    act_copy(1, 2, 1).start()
+    acc[2] += jnp.dot(acts[1, 2], wst_ref[...], preferred_element_type=F32)
+    give(2)
+    act_copy(1, 0, 1).wait_recv()
+    acc[1] += jnp.dot(acts[1, 1], wst_ref[...], preferred_element_type=F32)
+    give(1)
+    finish(0)
+    finish(2)
+    finish(1)
+    act_copy(1, 2, 1).wait_recv()
+    acc[3] += jnp.dot(acts[1, 3], wst_ref[...], preferred_element_type=F32)
+    give(3)
+    finish(3)
+    for d in (2, 1, 3):
+        sum_copy(d).wait_recv()
+        out_ref[0, :, pl.ds(pl.multiple_of((f ^ d) * cols, cols), cols)] = landed[d]
+
+    @pl.when(me < sp - 1)
+    def _():
+        for copy in tail:
+            copy.wait_send()
+
+    for d in range(1, sp):
+
+        @pl.when(me + d < sp)
+        def _(d=d):
+            for copy in kv_copies(d, me) + st_copies(d, me):
+                copy.wait_send()
+
+    for kind, via in ((0, 1), (1, 2)):
+        act_copy(kind, 0, 1).wait_send()
+        act_copy(kind, 0, 2).wait_send()
+        act_copy(kind, via, 3 ^ via).wait_send()
+    for d in range(fs):
+        half_copy(d).wait_send()
+    for d in range(1, fs):
+        sum_copy(d).wait_send()
+
+
+def fused(sp, fs, *args):
+    x, w = args[0], args[1]
+    rows, width = x.shape[1], x.shape[2]
+    heads = args[4].shape[1]
+    cols = args[16].shape[1]
+    half = rows // 2
+    args = list(args)
+    args[11] = args[11].reshape(1, -1)
+    vmem = pl.BlockSpec(memory_space=pltpu.VMEM)
+    smem = pl.BlockSpec(memory_space=pltpu.SMEM)
+    specs = [smem if i in (6, 7) else vmem for i in range(len(args))]
+    dma = pltpu.SemaphoreType.DMA
+    kv_width = args[13].shape[2]
+    kv_heads = kv_width // HEAD_DIM
+    return pl.pallas_call(
+        functools.partial(mixer_kernel, sp, fs),
+        out_shape=jax.ShapeDtypeStruct((1, half, cols * fs), BF16),
+        in_specs=specs,
+        out_specs=vmem,
+        scratch_shapes=[
+            pltpu.VMEM((8 + rows, width), F32),
+            pltpu.VMEM((16, width), BF16),
+            pltpu.VMEM((16, w.shape[2]), BF16),
+            pltpu.VMEM((16, w.shape[2]), BF16),
+            pltpu.VMEM((sp, rows, kv_width), BF16),
+            pltpu.VMEM((sp, rows, kv_width), BF16),
+            pltpu.VMEM((sp, heads, rows), F32),
+            pltpu.VMEM((kv_heads, heads // kv_heads * rows, kv_width), BF16),
+            pltpu.VMEM((sp, STATE, width), BF16),
+            pltpu.VMEM((sp, heads, LANES), F32),
+            pltpu.VMEM((STATE, width), F32),
+            pltpu.VMEM((rows, width), F32),
+            pltpu.VMEM((2, fs, rows, width), BF16),
+            pltpu.VMEM((fs, rows, cols), F32),
+            pltpu.VMEM((fs, half, cols), BF16),
+            pltpu.VMEM((fs, half, cols), BF16),
+            pltpu.VMEM((fs, half, cols), BF16),
+            pltpu.VMEM((fs, half, cols), BF16),
+            dma((3,)),
+            dma((3,)),
+            dma((sp, 3)),
+            dma((sp, 3)),
+            dma((sp, 2)),
+            dma((sp, 2)),
+            dma((2, fs)),
+            dma((2, fs)),
+            dma((fs,)),
+            dma((fs,)),
+            dma((fs,)),
+            dma((fs,)),
+        ],
+        compiler_params=pltpu.CompilerParams(collective_id=0, has_side_effects=True),
+    )(*args)
+
+
+def one_kernel(*args, sp, fs, tp):
+    rows, width = args[0].shape[1:]
+    heads = args[4].shape[1]
+    return (
+        1 < sp <= 8
+        and fs == 4
+        and tp == 2
+        and rows == LANES
+        and args[1].shape[2] == STATE
+        and width == heads * HEAD_DIM
+        and args[12].shape[2] == width
+        and args[13].shape[2] == 2 * HEAD_DIM
+        and heads % 4 == 0
+    )
+
+
 def solution(mesh):
     in_specs = (
         P("fs", "sp", "tp"),
@@ -258,4 +720,11 @@
         P("tp", "fs"),
     )
     out_specs = P("fs", ("sp", "tp"), None)
-    return jax.shard_map(shards, mesh=mesh, in_specs=in_specs, out_specs=out_specs, check_vma=False)
+    sp, fs, tp = (mesh.shape[name] for name in ("sp", "fs", "tp"))
+
+    def body(*args):
+        if one_kernel(*args, sp=sp, fs=fs, tp=tp):
+            return fused(sp, fs, *args)
+        return shards(*args)
+
+    return jax.shard_map(body, mesh=mesh, in_specs=in_specs, out_specs=out_specs, check_vma=False)

time: 109 us -> 41 us (0.38)
  blocking collectives: 49.9 us -> 0 us
  Pallas kernels: 0 us -> 37.5 us
  waiting for transfers between devices: 22.8 us -> 0 us
  between operations: 14 us -> 0.01 us
  other arithmetic: 7.12 us -> 0 us
  matrix products: 7.04 us -> 0 us
  local copies, waits for them, and re-layouts: 5.14 us -> 3.08 us
  starting transfers between devices: 1.37 us -> 0 us
    all_gather x4 -> x0, blocking collectives: 41.6 us -> none  [the longest x1 12 us: entering(): lax.all_gather(a.astype(kind), axis)]
    pallas_call x0 -> x1, Pallas kernels: none -> 37.5 us  [fused(): pl.pallas_call(functools.partial(mixer_kernel, sp, fs), out_shape=jax.Sha...]
    reduce_scatter x1 -> x0, waiting for transfers between devices: 16.1 us -> none  [shards(): lax.psum_scatter((jnp.dot(state_result, state_columns, preferred_element_...]
    unnamed x1 -> x0, blocking collectives: 8.25 us -> none
    dot_general x8 -> x0, matrix products: 7.04 us -> none  [the longest x1 2.87 us: shards(): jnp.dot(attend_out, attend_columns, preferred_element_type=jnp.float32)]
    all_gather x2 -> x0, waiting for transfers between devices: 5.92 us -> none  [the longest x1 5.9 us: shards(): lax.all_gather(attention_out_weight, 'fs', axis=1, tiled=True)]
    mul x3 -> x0, other arithmetic: 2.52 us -> none  [causal_filter(): taps[offset].astype(jnp.float32) * padded[offset:offset + length]]
    slice x7 -> x0, local copies, waits for them, and re-layouts: 1.77 us -> none  [the longest x1 0.71 us: shards(): read_rows[-tap_rows:]]
  transfers between devices with their start and end apart: 4 -> 0, of which waited for: 2 -> 0; matrix products, arithmetic and copies ran while one was open for 15% -> 0% of each run, Pallas kernels for 0% -> 0%
where the time goes in v1:
time: 41 us; the launch traced here: 40.5 us
  Pallas kernels  37.5 us (91%)
  local copies, waits for them, and re-layouts  3.08 us (8%)
    pallas_call x1, Pallas kernels, fused(): pl.pallas_call(functools.partial(mixer_kernel, sp, fs), out_shape=jax.Sha...  37.5 us
    unnamed x2, local copies, waits for them, and re-layouts  3.08 us

profile of v1, /device:TPU:25, one launch (start us, length us, event | category | flops | bytes accessed | tf_op | source)
XLA Modules:
  0.0 40.5 jit_solution(10713141792423753352)
XLA Ops:
  0.0 1.4 %copy.19.forget_ref = f32[1,128,8]{2,1,0:T(8,128)} copy(f32[1,128,8]{1,2,0:T(8,128)} %param.33) | data formatting | bytes 8192 | tf_op args[15]
  1.4 37.5 %shard_map.172 = bf16[1,64,2048]{2,1,0:T(8,128)(2,1)} custom-call(bf16[1,128,512]{2,1,0:T(8,128)(2,1)} %x_ref.1, bf16[1,128,128]{2,1,0:T(8,128)(2,1)} %w_ref.1, bf16[1,128,128]{2,1,0:T(8,128)(2,1)} %r_ref.1, bf16[1,128,512]{2,1,0:T(8,128)(2,1)} %gate_ref.1, f32[1,8,128]{2,1,0:T(8,128)} %step_ref.1, f32[1,8,128]{2,1,0:T(8,128)} %extra_ref.1, f32[8]{0:T(128)} %shrink_ref.1, ...), custom_call_target="tpu_custom_call" | custom-call | tf_op jit(solution)/shard_map/pallas_call | solution.py:644
  38.9 1.7 %copy.21 = bf16[1,64,2048]{2,1,0:T(8,128)(2,1)} copy(bf16[1,64,2048]{2,1,0:T(8,128)(2,1)} %shard_map.172) | data formatting | bytes 524288

commit v2 on v1

--- a/solution.py
+++ b/solution.py
@@ -267,9 +267,9 @@
     wat_ref,
     out_ref,
     pad_ref,
-    tailx,
-    tailw,
-    tailr,
+    tails,
+    conv,
+    end_wide,
     kall,
     vall,
     gall,
@@ -279,7 +279,10 @@
     carried,
     mix,
     acts,
+    pieces,
+    scales,
     acc,
+    acc_state,
     half_out,
     half_in,
     sums,
@@ -292,6 +295,8 @@
     st_recv,
     act_send,
     act_recv,
+    piece_send,
+    piece_recv,
     half_send,
     half_recv,
     sum_send,
@@ -330,64 +335,37 @@
             device_id_type=MESH,
         )
 
-    gall[me] = forget_ref[0].T
-    kall[me] = k_ref[0]
-    vall[me] = v_ref[0]
-    pl.semaphore_wait(barrier, sp - 1 + fs - 1 + 1)
-
-    tail = [
-        remote(
-            src.at[0, rows - 16 : rows, :],
-            dst,
-            tail_send.at[i],
-            tail_recv.at[i],
-            {"sp": lax.rem(me + 1, sp)},
-        )
-        for i, (src, dst) in enumerate(((x_ref, tailx), (w_ref, tailw), (r_ref, tailr)))
-    ]
-
-    @pl.when(me < sp - 1)
-    def _():
-        for copy in tail:
-            copy.start()
-
-    def kv_copies(d, source):
-        there = {"sp": lax.rem(me + d, sp)}
-        return [
-            remote(src, dst.at[source], kv_send.at[d, i], kv_recv.at[source, i], there)
-            for i, (src, dst) in enumerate(
-                ((k_ref.at[0], kall), (v_ref.at[0], vall), (gall.at[me], gall))
-            )
-        ]
-
-    for d in range(1, sp):
-
-        @pl.when(me + d < sp)
-        def _(d=d):
-            for copy in kv_copies(d, me):
-                copy.start()
-
     lane = lax.broadcasted_iota(jnp.int32, (1, LANES), 1)
     low = lane < HEAD_DIM
     row_id = lax.broadcasted_iota(jnp.int32, (rows, rows), 0)
     col_id = lax.broadcasted_iota(jnp.int32, (rows, rows), 1)
 
-    for j in range(1, sp):
-
-        @pl.when(j > me)
-        def _(j=j):
-            kall[j] = jnp.zeros(kall.shape[1:], BF16)
-            vall[j] = jnp.zeros(vall.shape[1:], BF16)
-            gall[j] = jnp.zeros(gall.shape[1:], F32)
-
-    for h in range(heads):
-        kv = h // repeat
-        piece = (q_ref[0, :, h * HEAD_DIM : (h + 1) * HEAD_DIM].astype(F32) * HEAD_DIM**-0.5).astype(
-            BF16
-        )
-        zero = jnp.zeros((rows, HEAD_DIM), BF16)
-        parts = [piece if i == kv else zero for i in range(kv_heads)]
-        qs[kv, (h % repeat) * rows : (h % repeat + 1) * rows, :] = jnp.concatenate(parts, axis=1)
+    def expand(columns, j):
+        return jnp.where(low, columns[:, 2 * j : 2 * j + 1], columns[:, 2 * j + 1 : 2 * j + 2])
+
+    gall[me] = forget_ref[0]
+    gate_cols = forget_ref[0].T
+    kall[me] = k_ref[0]
+    vall[me] = v_ref[0]
+
+    inputs = (
+        (x_ref, tapx_ref, slice(0, width)),
+        (w_ref, tapw_ref, slice(width, width + STATE)),
+        (r_ref, tapr_ref, slice(width + STATE, width + 2 * STATE)),
+    )
+
+    def filtered(count):
+        for _, tap_ref, at in inputs:
+            total = jnp.zeros((count, at.stop - at.start), F32)
+            for i in range(taps):
+                first = 8 - (taps - 1) + i
+                total = total + tap_ref[i : i + 1, :].astype(F32) * pad_ref[first : first + count, at]
+            conv[0:count, at] = (total * jax.nn.sigmoid(total)).astype(BF16)
+
+    pad_ref[0:8, :] = jnp.zeros((8, pad_ref.shape[1]), F32)
+    for ref, _, at in inputs:
+        pad_ref[8 : 8 + rows, at] = ref[0].astype(F32)
+    filtered(rows)
 
     head_row = lax.broadcasted_iota(jnp.int32, (heads, rows), 0)
     power = jnp.zeros((heads, rows), F32)
@@ -399,75 +377,88 @@
     upper = (row_id <= col_id).astype(F32)
     cum = jnp.dot(log_decay, upper, precision=lax.Precision.HIGHEST, preferred_element_type=F32)
     cum_end = cum[:, rows - 1 : rows]
+    decays[me] = jnp.broadcast_to(jnp.exp(cum_end), (heads, LANES))
     end_scale = (jnp.exp(cum_end - cum) * step).T
-    exp_cum = jnp.exp(cum).T
-    cum_col = cum.T
-    decays[me] = jnp.broadcast_to(jnp.exp(cum_end), (heads, LANES))
+    for j in range(pairs):
+        end_wide[:, j * LANES : (j + 1) * LANES] = expand(end_scale, j)
+
+    pl.semaphore_wait(barrier, sp - 1 + fs - 1 + 1)
+
+    tail = [
+        remote(
+            ref.at[0, rows - 16 : rows, :],
+            tails.at[:, at],
+            tail_send.at[i],
+            tail_recv.at[i],
+            {"sp": lax.rem(me + 1, sp)},
+        )
+        for i, (ref, _, at) in enumerate(inputs)
+    ]
+
+    @pl.when(me < sp - 1)
+    def _():
+        for copy in tail:
+            copy.start()
+
+    def kv_copies(d, source):
+        there = {"sp": lax.rem(me + d, sp)}
+        return [
+            remote(src, dst.at[source], kv_send.at[d, i], kv_recv.at[source, i], there)
+            for i, (src, dst) in enumerate(
+                ((k_ref.at[0], kall), (v_ref.at[0], vall), (gall.at[me], gall))
+            )
+        ]
+
+    for d in range(1, sp):
+
+        @pl.when(me + d < sp)
+        def _(d=d):
+            for copy in kv_copies(d, me):
+                copy.start()
+
+    for j in range(1, sp):
+
+        @pl.when(j > me)
+        def _(j=j):
+            kall[j] = jnp.zeros(kall.shape[1:], BF16)
+            vall[j] = jnp.zeros(vall.shape[1:], BF16)
+            gall[j] = jnp.zeros(gall.shape[1:], F32)
+
+    for h in range(heads):
+        kv = h // repeat
+        piece = (q_ref[0, :, h * HEAD_DIM : (h + 1) * HEAD_DIM].astype(F32) * HEAD_DIM**-0.5).astype(
+            BF16
+        )
+        zero = jnp.zeros((rows, HEAD_DIM), BF16)
+        parts = [piece if i == kv else zero for i in range(kv_heads)]
+        qs[kv, (h % repeat) * rows : (h % repeat + 1) * rows, :] = jnp.concatenate(parts, axis=1)
 
     @pl.when(me > 0)
     def _():
         for copy in tail:
             copy.wait_recv()
 
-    def filtered(ref, tail_ref, tap_ref, n):
-        before = jnp.where(me > 0, tail_ref[...].astype(F32)[8:16], 0.0)
-        pad_ref[0:8, 0:n] = before
-        pad_ref[8 : 8 + rows, 0:n] = ref[0].astype(F32)
-        total = jnp.zeros((rows, n), F32)
-        for i in range(taps):
-            at = 8 - (taps - 1) + i
-            total = total + tap_ref[i : i + 1, :].astype(F32) * pad_ref[at : at + rows, 0:n]
-        return (total * jax.nn.sigmoid(total)).astype(BF16)
-
-    conv_write = filtered(w_ref, tailw, tapw_ref, STATE)
-    conv_values = filtered(x_ref, tailx, tapx_ref, width)
-
-    def expand(columns, j):
-        return jnp.where(low, columns[:, 2 * j : 2 * j + 1], columns[:, 2 * j + 1 : 2 * j + 2])
-
-    weighted = jnp.concatenate(
-        [
-            (
-                conv_values[:, j * LANES : (j + 1) * LANES].astype(F32) * expand(end_scale, j)
-            ).astype(BF16)
-            for j in range(pairs)
-        ],
-        axis=1,
-    )
-    states[me] = lax.dot_general(
-        conv_write, weighted, (((0,), (0,)), ((), ())), preferred_element_type=F32
-    ).astype(BF16)
-
-    def st_copies(d, source):
+    pad_ref[0:8, :] = jnp.where(me > 0, tails[...].astype(F32)[8:16], 0.0)
+    filtered(16)
+    conv_write = conv[:, width : width + STATE]
+    turned_write = conv_write.astype(F32).T.astype(BF16)
+
+    def st_copy(d, source, p):
         there = {"sp": lax.rem(me + d, sp)}
-        return [
-            remote(buf.at[source], buf.at[source], st_send.at[d, i], st_recv.at[source, i], there)
-            for i, buf in enumerate((states, decays))
-        ]
-
-    for d in range(1, sp):
-
-        @pl.when(me + d < sp)
-        def _(d=d):
-            for copy in st_copies(d, me):
-                copy.start()
-
-    conv_read = filtered(r_ref, tailr, tapr_ref, STATE)
-    inner = lax.dot_general(
-        conv_read, conv_write, (((1,), (1,)), ((), ())), preferred_element_type=F32
-    )
-    causal = row_id >= col_id
-    for j in range(pairs):
-        tile = conv_values[:, j * LANES : (j + 1) * LANES]
-        parts = []
-        for h in (2 * j, 2 * j + 1):
-            gap = jnp.where(causal, cum_col[:, h : h + 1] - cum[h : h + 1, :], NEGATIVE)
-            weights = (inner * (jnp.exp(gap) * step[h : h + 1, :])).astype(BF16)
-            parts.append(jnp.dot(weights, tile, preferred_element_type=F32))
-        bypass = jnp.where(low, bypass_ref[2 * j], bypass_ref[2 * j + 1])
-        mix[:, j * LANES : (j + 1) * LANES] = (
-            jnp.where(low, parts[0], parts[1]) + bypass * tile.astype(F32)
-        )
+        ref = states.at[source, p] if p < pairs else decays.at[source]
+        return remote(ref, ref, st_send.at[d, p], st_recv.at[source, p], there)
+
+    for p in range(pairs):
+        at = slice(p * LANES, (p + 1) * LANES)
+        weighted = (conv[:, at].astype(F32) * end_wide[:, at]).astype(BF16)
+        states[me, p] = jnp.dot(turned_write, weighted, preferred_element_type=F32).astype(BF16)
+        for d in range(1, sp):
+
+            @pl.when(me + d < sp)
+            def _(d=d, p=p):
+                if p == 0:
+                    st_copy(d, me, pairs).start()
+                st_copy(d, me, p).start()
 
     for j in range(sp - 1):
 
@@ -488,7 +479,7 @@
         outs = []
         for i in range(repeat):
             h = kv * repeat + i
-            gate_col = forget_ref[0, :, h : h + 1]
+            gate_col = gate_cols[:, h : h + 1]
             tiles = [
                 jnp.where(
                     visible[j],
@@ -508,55 +499,114 @@
             outs.append(both / turned if h % 2 == kv else turned / both)
         for i in range(0, repeat, 2):
             h = kv * repeat + i
-            acts[0, 0, :, h * HEAD_DIM : (h + 2) * HEAD_DIM] = jnp.where(
+            acts[0, :, h * HEAD_DIM : (h + 2) * HEAD_DIM] = jnp.where(
                 low, outs[i], outs[i + 1]
             ).astype(BF16)
 
-    def act_copy(kind, origin, hop):
+    def act_copy(origin, hop):
+        there = origin ^ hop
         return remote(
-            acts.at[kind, origin],
-            acts.at[kind, origin ^ hop],
-            act_send.at[kind, origin ^ hop],
-            act_recv.at[kind, origin ^ hop],
-            {"fs": lax.rem(f + 0, fs) ^ hop},
-        )
-
-    act_copy(0, 0, 1).start()
-    act_copy(0, 0, 2).start()
-    acc[0] = jnp.dot(acts[0, 0], wat_ref[...], preferred_element_type=F32)
-    act_copy(0, 0, 1).wait_recv()
-    act_copy(0, 1, 2).start()
-    acc[1] = jnp.dot(acts[0, 1], wat_ref[...], preferred_element_type=F32)
-
-    carried[...] = jnp.zeros(carried.shape, F32)
-    for j in range(sp - 1):
-
-        @pl.when(j < me)
-        def _(j=j):
-            for copy in st_copies(1, j):
-                copy.wait_recv()
-            for p in range(pairs):
-                at = slice(p * LANES, (p + 1) * LANES)
+            acts.at[origin],
+            acts.at[there],
+            act_send.at[there],
+            act_recv.at[there],
+            {"fs": f ^ hop},
+        )
+
+    def piece_copy(p, origin, hop):
+        there = origin ^ hop
+        ref = pieces if p < pairs else scales
+        index = (lambda slot: (p, slot)) if p < pairs else (lambda slot: (slot,))
+        return remote(
+            ref.at[index(origin)],
+            ref.at[index(there)],
+            piece_send.at[p, there],
+            piece_recv.at[p, there],
+            {"fs": f ^ hop},
+        )
+
+    act_copy(0, 1).start()
+    act_copy(0, 2).start()
+
+    exp_cum = jnp.exp(cum).T
+    cum_col = cum.T
+    conv_read = conv[:, width + STATE :]
+    inner = lax.dot_general(
+        conv_read, conv_write, (((1,), (1,)), ((), ())), preferred_element_type=F32
+    )
+    causal = row_id >= col_id
+    for j in range(pairs):
+        tile = conv[:, j * LANES : (j + 1) * LANES]
+        parts = []
+        for h in (2 * j, 2 * j + 1):
+            gap = jnp.where(causal, cum_col[:, h : h + 1] - cum[h : h + 1, :], NEGATIVE)
+            weights = (inner * (jnp.exp(gap) * step[h : h + 1, :])).astype(BF16)
+            parts.append(jnp.dot(weights, tile, preferred_element_type=F32))
+        bypass = jnp.where(low, bypass_ref[2 * j], bypass_ref[2 * j + 1])
+        mix[:, j * LANES : (j + 1) * LANES] = (
+            jnp.where(low, parts[0], parts[1]) + bypass * tile.astype(F32)
+        )
+
+    @pl.when(me > 0)
+    def _():
+        for j in range(sp - 1):
+
+            @pl.when(j < me)
+            def _(j=j):
+                st_copy(1, j, pairs).wait_recv()
+
+    squares = []
+
+    def piece(p):
+        at = slice(p * LANES, (p + 1) * LANES)
+        carried[...] = jnp.zeros(carried.shape, F32)
+        for j in range(sp - 1):
+
+            @pl.when(j < me)
+            def _(j=j):
+                st_copy(1, j, p).wait_recv()
                 decay = jnp.where(
                     low, decays[j, 2 * p : 2 * p + 1, :], decays[j, 2 * p + 1 : 2 * p + 2, :]
                 )
-                carried[:, at] = carried[:, at] * decay + states[j, :, at].astype(F32)
-
-    entered = jnp.dot(conv_read, carried[...].astype(BF16), preferred_element_type=F32)
-    squares = jnp.zeros((rows, LANES), F32)
-    gated = []
+                carried[...] = carried[...] * decay + states[j, p].astype(F32)
+
+        entered = jnp.dot(conv_read, carried[...].astype(BF16), preferred_element_type=F32)
+        gate = gate_ref[0, :, at].astype(F32)
+        u = (mix[:, at] + entered * expand(exp_cum, p)) * (gate * jax.nn.sigmoid(gate))
+        squares.append(u * u)
+        pieces[p, 0] = (u * gain_ref[0:1, at]).astype(BF16)
+        piece_copy(p, 0, 2).start()
+        piece_copy(p, 0, 1).start()
+        if p == pairs - 1:
+            piece_copy(p, 0, 3).start()
+
+    def pass_on(p):
+        piece_copy(p, 0, 2).wait_recv()
+        piece_copy(p, 2, 1).start()
+
     for p in range(pairs):
-        at = slice(p * LANES, (p + 1) * LANES)
-        gate = gate_ref[0, :, at].astype(F32)
-        u = (mix[:, at] + entered[:, at] * expand(exp_cum, p)) * (gate * jax.nn.sigmoid(gate))
-        gated.append(u)
-        squares = squares + u * u
-    scale = lax.rsqrt(jnp.sum(squares, axis=1, keepdims=True) / width + EPSILON)
-    for p in range(pairs):
-        at = slice(p * LANES, (p + 1) * LANES)
-        acts[1, 0, :, at] = (gated[p] * scale * gain_ref[0:1, at]).astype(BF16)
-    act_copy(1, 0, 2).start()
-    act_copy(1, 0, 1).start()
+        piece(p)
+        if p == pairs - 1:
+            total = functools.reduce(jnp.add, squares)
+            ones = jnp.ones((8, LANES), F32)
+            mean = (
+                lax.dot_general(
+                    ones,
+                    total,
+                    (((1,), (1,)), ((), ())),
+                    precision=lax.Precision.HIGHEST,
+                    preferred_element_type=F32,
+                )
+                / width
+            )
+            scales[0] = lax.rsqrt(mean + EPSILON)
+            for d in range(1, fs):
+                piece_copy(pairs, 0, d).start()
+        if p == min(1, pairs - 1):
+            act_copy(0, 1).wait_recv()
+            act_copy(1, 2).start()
+        if p >= 1:
+            pass_on(p - 1)
 
     def half_copy(d):
         return remote(
@@ -581,25 +631,36 @@
         else:
             out_ref[0, :, pl.ds(pl.multiple_of(f * cols, cols), cols)] = total
 
-    acc[0] += jnp.dot(acts[1, 0], wst_ref[...], preferred_element_type=F32)
-    give(0)
-    act_copy(0, 0, 2).wait_recv()
-    acc[2] = jnp.dot(acts[0, 2], wat_ref[...], preferred_element_type=F32)
-    act_copy(0, 1, 2).wait_recv()
-    acc[3] = jnp.dot(acts[0, 3], wat_ref[...], preferred_element_type=F32)
-    act_copy(1, 0, 2).wait_recv()
-    act_copy(1, 2, 1).start()
-    acc[2] += jnp.dot(acts[1, 2], wst_ref[...], preferred_element_type=F32)
-    give(2)
-    act_copy(1, 0, 1).wait_recv()
-    acc[1] += jnp.dot(acts[1, 1], wst_ref[...], preferred_element_type=F32)
-    give(1)
-    finish(0)
+    cut = (pairs - 1) * LANES
+
+    def most(d):
+        first = jnp.concatenate([pieces[p, d] for p in range(pairs - 1)], axis=1)
+        acc[d] = jnp.dot(acts[d], wat_ref[...], preferred_element_type=F32)
+        acc_state[d] = jnp.dot(first, wst_ref[0:cut, :], preferred_element_type=F32)
+
+    def rest(d):
+        last = jnp.dot(pieces[pairs - 1, d], wst_ref[cut:, :], preferred_element_type=F32)
+        acc[d] += (acc_state[d] + last) * scales[d].T[:, 0:1]
+        give(d)
+
+    most(0)
+    rest(0)
+    act_copy(0, 2).wait_recv()
+    most(2)
+    act_copy(1, 2).wait_recv()
+    for p in range(pairs - 1):
+        piece_copy(p, 0, 1).wait_recv()
+        piece_copy(p, 2, 1).wait_recv()
+    most(1)
+    most(3)
+    for d in (2, 1, 3):
+        piece_copy(pairs - 1, 0, d).wait_recv()
+        piece_copy(pairs, 0, d).wait_recv()
+        rest(d)
+        if d == 2:
+            finish(0)
     finish(2)
     finish(1)
-    act_copy(1, 2, 1).wait_recv()
-    acc[3] += jnp.dot(acts[1, 3], wst_ref[...], preferred_element_type=F32)
-    give(3)
     finish(3)
     for d in (2, 1, 3):
         sum_copy(d).wait_recv()
@@ -614,13 +675,18 @@
 
         @pl.when(me + d < sp)
         def _(d=d):
-            for copy in kv_copies(d, me) + st_copies(d, me):
+            for copy in kv_copies(d, me) + [st_copy(d, me, p) for p in range(pairs + 1)]:
                 copy.wait_send()
 
-    for kind, via in ((0, 1), (1, 2)):
-        act_copy(kind, 0, 1).wait_send()
-        act_copy(kind, 0, 2).wait_send()
-        act_copy(kind, via, 3 ^ via).wait_send()
+    for hop, origin in ((1, 0), (2, 0), (2, 1)):
+        act_copy(origin, hop).wait_send()
+    for p in range(pairs + 1):
+        piece_copy(p, 0, 1).wait_send()
+        piece_copy(p, 0, 2).wait_send()
+        if p < pairs - 1:
+            piece_copy(p, 2, 1).wait_send()
+        else:
+            piece_copy(p, 0, 3).wait_send()
     for d in range(fs):
         half_copy(d).wait_send()
     for d in range(1, fs):
@@ -635,6 +701,7 @@
     half = rows // 2
     args = list(args)
     args[11] = args[11].reshape(1, -1)
+    args[15] = jnp.swapaxes(args[15], 1, 2)
     vmem = pl.BlockSpec(memory_space=pltpu.VMEM)
     smem = pl.BlockSpec(memory_space=pltpu.SMEM)
     specs = [smem if i in (6, 7) else vmem for i in range(len(args))]
@@ -647,19 +714,22 @@
         in_specs=specs,
         out_specs=vmem,
         scratch_shapes=[
-            pltpu.VMEM((8 + rows, width), F32),
-            pltpu.VMEM((16, width), BF16),
-            pltpu.VMEM((16, w.shape[2]), BF16),
-            pltpu.VMEM((16, w.shape[2]), BF16),
+            pltpu.VMEM((8 + rows, width + 2 * STATE), F32),
+            pltpu.VMEM((16, width + 2 * STATE), BF16),
+            pltpu.VMEM((rows, width + 2 * STATE), BF16),
+            pltpu.VMEM((rows, width), F32),
             pltpu.VMEM((sp, rows, kv_width), BF16),
             pltpu.VMEM((sp, rows, kv_width), BF16),
             pltpu.VMEM((sp, heads, rows), F32),
             pltpu.VMEM((kv_heads, heads // kv_heads * rows, kv_width), BF16),
-            pltpu.VMEM((sp, STATE, width), BF16),
+            pltpu.VMEM((sp, heads // 2, STATE, LANES), BF16),
             pltpu.VMEM((sp, heads, LANES), F32),
-            pltpu.VMEM((STATE, width), F32),
+            pltpu.VMEM((STATE, LANES), F32),
             pltpu.VMEM((rows, width), F32),
-            pltpu.VMEM((2, fs, rows, width), BF16),
+            pltpu.VMEM((fs, rows, width), BF16),
+            pltpu.VMEM((heads // 2, fs, rows, LANES), BF16),
+            pltpu.VMEM((fs, 8, rows), F32),
+            pltpu.VMEM((fs, rows, cols), F32),
             pltpu.VMEM((fs, rows, cols), F32),
             pltpu.VMEM((fs, half, cols), BF16),
             pltpu.VMEM((fs, half, cols), BF16),
@@ -669,10 +739,12 @@
             dma((3,)),
             dma((sp, 3)),
             dma((sp, 3)),
-            dma((sp, 2)),
-            dma((sp, 2)),
-            dma((2, fs)),
-            dma((2, fs)),
+            dma((sp, heads // 2 + 1)),
+            dma((sp, heads // 2 + 1)),
+            dma((fs,)),
+            dma((fs,)),
+            dma((heads // 2 + 1, fs)),
+            dma((heads // 2 + 1, fs)),
             dma((fs,)),
             dma((fs,)),
             dma((fs,)),
@@ -690,7 +762,7 @@
         and fs == 4
         and tp == 2
         and rows == LANES
-        and args[1].shape[2] == STATE
+        and args[1].shape[2] == STATE == LANES
         and width == heads * HEAD_DIM
         and args[12].shape[2] == width
         and args[13].shape[2] == 2 * HEAD_DIM

time: 41 us -> 40.3 us (0.983)
  local copies, waits for them, and re-layouts: 3.08 us -> 1.67 us
  Pallas kernels: 37.5 us -> 38.5 us
    unnamed x2 -> x1, local copies, waits for them, and re-layouts: 3.08 us -> 1.67 us
    pallas_call x1, Pallas kernels: 37.5 us -> 38.5 us  [fused(): pl.pallas_call(functools.partial(mixer_kernel, sp, fs), out_shape=jax.Sha...]
where the time goes in v2:
time: 40.3 us; the launch traced here: 40.2 us
  Pallas kernels  38.5 us (96%)
  local copies, waits for them, and re-layouts  1.67 us (4%)
    pallas_call x1, Pallas kernels, fused(): pl.pallas_call(functools.partial(mixer_kernel, sp, fs), out_shape=jax.Sha...  38.5 us
    unnamed x1, local copies, waits for them, and re-layouts  1.67 us

profile of v2, /device:TPU:25, one launch (start us, length us, event | category | flops | bytes accessed | tf_op | source)
XLA Modules:
  0.0 40.2 jit_solution(11988013057061520071)
XLA Ops:
  0.0 38.5 %shard_map.172 = bf16[1,64,2048]{2,1,0:T(8,128)(2,1)} custom-call(bf16[1,128,512]{2,1,0:T(8,128)(2,1)} %x_ref.1, bf16[1,128,128]{2,1,0:T(8,128)(2,1)} %w_ref.1, bf16[1,128,128]{2,1,0:T(8,128)(2,1)} %r_ref.1, bf16[1,128,512]{2,1,0:T(8,128)(2,1)} %gate_ref.1, f32[1,8,128]{2,1,0:T(8,128)} %step_ref.1, f32[1,8,128]{2,1,0:T(8,128)} %extra_ref.1, f32[8]{0:T(128)} %shrink_ref.1, ...), custom_call_target="tpu_custom_call" | custom-call | tf_op jit(solution)/shard_map/pallas_call | solution.py:711
  38.5 1.7 %copy.20 = bf16[1,64,2048]{2,1,0:T(8,128)(2,1)} copy(bf16[1,64,2048]{2,1,0:T(8,128)(2,1)} %shard_map.172) | data formatting | bytes 524288

commit v3 on v2

--- a/solution.py
+++ b/solution.py
@@ -274,9 +274,9 @@
     vall,
     gall,
     qs,
-    states,
-    decays,
-    carried,
+    own_state,
+    state_in,
+    state_out,
     mix,
     acts,
     pieces,
@@ -377,7 +377,12 @@
     upper = (row_id <= col_id).astype(F32)
     cum = jnp.dot(log_decay, upper, precision=lax.Precision.HIGHEST, preferred_element_type=F32)
     cum_end = cum[:, rows - 1 : rows]
-    decays[me] = jnp.broadcast_to(jnp.exp(cum_end), (heads, LANES))
+    decays = jnp.broadcast_to(jnp.exp(cum_end), (heads, LANES))
+
+    @pl.when(me == 0)
+    def _():
+        state_in[...] = jnp.zeros(state_in.shape, BF16)
+
     end_scale = (jnp.exp(cum_end - cum) * step).T
     for j in range(pairs):
         end_wide[:, j * LANES : (j + 1) * LANES] = expand(end_scale, j)
@@ -443,22 +448,19 @@
     conv_write = conv[:, width : width + STATE]
     turned_write = conv_write.astype(F32).T.astype(BF16)
 
-    def st_copy(d, source, p):
-        there = {"sp": lax.rem(me + d, sp)}
-        ref = states.at[source, p] if p < pairs else decays.at[source]
-        return remote(ref, ref, st_send.at[d, p], st_recv.at[source, p], there)
+    def st_copy(p):
+        there = {"sp": lax.rem(me + 1, sp)}
+        return remote(state_out.at[p], state_in.at[p], st_send.at[p], st_recv.at[p], there)
 
     for p in range(pairs):
         at = slice(p * LANES, (p + 1) * LANES)
         weighted = (conv[:, at].astype(F32) * end_wide[:, at]).astype(BF16)
-        states[me, p] = jnp.dot(turned_write, weighted, preferred_element_type=F32).astype(BF16)
-        for d in range(1, sp):
-
-            @pl.when(me + d < sp)
-            def _(d=d, p=p):
-                if p == 0:
-                    st_copy(d, me, pairs).start()
-                st_copy(d, me, p).start()
+        own_state[p] = jnp.dot(turned_write, weighted, preferred_element_type=F32)
+
+        @pl.when(me == 0)
+        def _(p=p):
+            state_out[p] = own_state[p].astype(BF16)
+            st_copy(p).start()
 
     for j in range(sp - 1):
 
@@ -528,6 +530,14 @@
     act_copy(0, 1).start()
     act_copy(0, 2).start()
 
+    @pl.when(jnp.logical_and(me > 0, me < sp - 1))
+    def _():
+        for p in range(pairs):
+            st_copy(p).wait_recv()
+            decay = jnp.where(low, decays[2 * p : 2 * p + 1, :], decays[2 * p + 1 : 2 * p + 2, :])
+            state_out[p] = (state_in[p].astype(F32) * decay + own_state[p]).astype(BF16)
+            st_copy(p).start()
+
     exp_cum = jnp.exp(cum).T
     cum_col = cum.T
     conv_read = conv[:, width + STATE :]
@@ -547,30 +557,16 @@
             jnp.where(low, parts[0], parts[1]) + bypass * tile.astype(F32)
         )
 
-    @pl.when(me > 0)
-    def _():
-        for j in range(sp - 1):
-
-            @pl.when(j < me)
-            def _(j=j):
-                st_copy(1, j, pairs).wait_recv()
-
     squares = []
 
     def piece(p):
         at = slice(p * LANES, (p + 1) * LANES)
-        carried[...] = jnp.zeros(carried.shape, F32)
-        for j in range(sp - 1):
-
-            @pl.when(j < me)
-            def _(j=j):
-                st_copy(1, j, p).wait_recv()
-                decay = jnp.where(
-                    low, decays[j, 2 * p : 2 * p + 1, :], decays[j, 2 * p + 1 : 2 * p + 2, :]
-                )
-                carried[...] = carried[...] * decay + states[j, p].astype(F32)
-
-        entered = jnp.dot(conv_read, carried[...].astype(BF16), preferred_element_type=F32)
+
+        @pl.when(me == sp - 1)
+        def _():
+            st_copy(p).wait_recv()
+
+        entered = jnp.dot(conv_read, state_in[p], preferred_element_type=F32)
         gate = gate_ref[0, :, at].astype(F32)
         u = (mix[:, at] + entered * expand(exp_cum, p)) * (gate * jax.nn.sigmoid(gate))
         squares.append(u * u)
@@ -668,14 +664,14 @@
 
     @pl.when(me < sp - 1)
     def _():
-        for copy in tail:
+        for copy in tail + [st_copy(p) for p in range(pairs)]:
             copy.wait_send()
 
     for d in range(1, sp):
 
         @pl.when(me + d < sp)
         def _(d=d):
-            for copy in kv_copies(d, me) + [st_copy(d, me, p) for p in range(pairs + 1)]:
+            for copy in kv_copies(d, me):
                 copy.wait_send()
 
     for hop, origin in ((1, 0), (2, 0), (2, 1)):
@@ -722,9 +718,9 @@
             pltpu.VMEM((sp, rows, kv_width), BF16),
             pltpu.VMEM((sp, heads, rows), F32),
             pltpu.VMEM((kv_heads, heads // kv_heads * rows, kv_width), BF16),
-            pltpu.VMEM((sp, heads // 2, STATE, LANES), BF16),
-            pltpu.VMEM((sp, heads, LANES), F32),
-            pltpu.VMEM((STATE, LANES), F32),
+            pltpu.VMEM((heads // 2, STATE, LANES), F32),
+            pltpu.VMEM((heads // 2, STATE, LANES), BF16),
+            pltpu.VMEM((heads // 2, STATE, LANES), BF16),
             pltpu.VMEM((rows, width), F32),
             pltpu.VMEM((fs, rows, width), BF16),
             pltpu.VMEM((heads // 2, fs, rows, LANES), BF16),
@@ -739,8 +735,8 @@
             dma((3,)),
             dma((sp, 3)),
             dma((sp, 3)),
-            dma((sp, heads // 2 + 1)),
-            dma((sp, heads // 2 + 1)),
+            dma((heads // 2,)),
+            dma((heads // 2,)),
             dma((fs,)),
             dma((fs,)),
             dma((heads // 2 + 1, fs)),

time: 40.3 us -> 37.9 us (0.940)
  Pallas kernels: 38.5 us -> 36.1 us
    pallas_call x1, Pallas kernels: 38.5 us -> 36.1 us  [fused(): pl.pallas_call(functools.partial(mixer_kernel, sp, fs), out_shape=jax.Sha...]
where the time goes in v3:
time: 37.9 us; the launch traced here: 37.7 us
  Pallas kernels  36.1 us (95%)
  local copies, waits for them, and re-layouts  1.67 us (4%)
    pallas_call x1, Pallas kernels, fused(): pl.pallas_call(functools.partial(mixer_kernel, sp, fs), out_shape=jax.Sha...  36.1 us
    unnamed x1, local copies, waits for them, and re-layouts  1.67 us

profile of v3, /device:TPU:25, one launch (start us, length us, event | category | flops | bytes accessed | tf_op | source)
XLA Modules:
  0.0 37.7 jit_solution(755886878703186808)
XLA Ops:
  0.0 36.1 %shard_map.172 = bf16[1,64,2048]{2,1,0:T(8,128)(2,1)} custom-call(bf16[1,128,512]{2,1,0:T(8,128)(2,1)} %x_ref.1, bf16[1,128,128]{2,1,0:T(8,128)(2,1)} %w_ref.1, bf16[1,128,128]{2,1,0:T(8,128)(2,1)} %r_ref.1, bf16[1,128,512]{2,1,0:T(8,128)(2,1)} %gate_ref.1, f32[1,8,128]{2,1,0:T(8,128)} %step_ref.1, f32[1,8,128]{2,1,0:T(8,128)} %extra_ref.1, f32[8]{0:T(128)} %shrink_ref.1, ...), custom_call_target="tpu_custom_call" | custom-call | tf_op jit(solution)/shard_map/pallas_call | solution.py:707
  36.1 1.7 %copy.20 = bf16[1,64,2048]{2,1,0:T(8,128)(2,1)} copy(bf16[1,64,2048]{2,1,0:T(8,128)(2,1)} %shard_map.172) | data formatting | bytes 524288
